TPU v7x, 256 devices: a whole 4x4x8 slice. The times are simulated.
256 devices in a mesh: ep: 64 (over z, y, core), tp: 4 (over x).
Axes of the slice: x: 4, y: 4, z: 8, core: 2. Of those that a mesh axis runs over, the one named last changes fastest.
Arguments:
- queries: bfloat16 [32768, 2048], P('ep', 'tp'), may hold values from -6 to 6
- forget_pre: float32 [32768, 2048], P('ep', 'tp'), may hold values from -8 to 20
- value_in: bfloat16 [32768, 2048], P('ep', 'tp'), may hold values from -6 to 6
- out_gate: bfloat16 [32768, 2048], P('ep', 'tp'), may hold values from -6 to 6
- lower_bound: float32 [2048], P('tp'), may hold values from 0.5 to 0.8
- out_gain: float32 [128], replicated, may hold values from 0.1 to 1.9
- out_weight: bfloat16 [2048, 2048], P('tp'), may hold values from -0.125 to 0.125
- moe_tokens: bfloat16 [16384, 2048], P('ep'), may hold values from -6 to 6
- moe_gain: float32 [2048], replicated, may hold values from 0.1 to 1.9
- expert_ids: int32 [16384, 4], P('ep'), may hold values from 0 to 127, all different within a row; in each aligned block of 64 rows (0 to 63, 64 to 127, ...) at most 4 rows name the same one
- route_weights: float32 [16384, 4], P('ep'), may hold values from 0.1 to 1
- w_gate: bfloat16 [128, 2048, 1024], P('ep', None, 'tp'), may hold values from -0.125 to 0.125
- w_up: bfloat16 [128, 2048, 1024], P('ep', None, 'tp'), may hold values from -0.125 to 0.125
- w_down: bfloat16 [128, 1024, 2048], P('ep', 'tp'), may hold values from -0.1875 to 0.1875
Outputs:
- mixer_out: bfloat16 [32768, 2048], P(('ep', 'tp'))
- expert_out: bfloat16 [16384, 2048], P(('ep', 'tp'))
Inputs may be any that keep to these rules, and one draw needn't show every extreme that they name: `expert_ids`: each row names 4 different experts. In each aligned block of 64 rows no expert is named by more than 4 rows, and in some block some expert is named by exactly 4 rows.
All inputs are finite; a program needn't handle non-finite values.
Results may differ from a plain program's by a relative error of at most 0.01065.
Values may be sent and summed in bfloat16 or wider, within the bound.
No kernel may reach another device: no remote copies, remote signals or barrier semaphores. Data moves between devices by JAX's collectives and lax.ppermute only.
A program may use at most 128 MiB of HBM per device.

v0:
```python
import jax
import jax.numpy as jnp
from jax import lax
from jax.experimental import pallas as pl
from jax.experimental.pallas import tpu as pltpu
from jax.sharding import Mesh
from jax.sharding import PartitionSpec as P


HEAD_DIM = 128
BLOCK = 64
EP = ("ep_0", "ep_1", "ep_2")
EP_TP = ("ep_0", "ep_1", "ep_2", "tp")

EPS = 1e-06
HIGHEST = lax.Precision.HIGHEST


def rms_scale(values, gain):
    return values * lax.rsqrt(jnp.mean(values * values, axis=-1, keepdims=True) + EPS) * gain


def dot_nt(a, b, precision=HIGHEST):
    return lax.dot_general(
        a, b, (((1,), (1,)), ((), ())), precision=precision, preferred_element_type=jnp.float32
    )


def dot_tn(a, b, precision=HIGHEST):
    return lax.dot_general(
        a, b, (((0,), (0,)), ((), ())), precision=precision, preferred_element_type=jnp.float32
    )


def dot_nn(a, b, precision=HIGHEST):
    return lax.dot_general(
        a, b, (((1,), (0,)), ((), ())), precision=precision, preferred_element_type=jnp.float32
    )


def recurrence_kernel(q_ref, f_ref, v_ref, bound_ref, rec_ref, query_ref, state_ref, decay_ref):
    rows = q_ref.shape[0]
    row = lax.broadcasted_iota(jnp.int32, (BLOCK, BLOCK), 0)
    col = lax.broadcasted_iota(jnp.int32, (BLOCK, BLOCK), 1)
    causal = row >= col
    lower = causal.astype(jnp.float32)
    scale = 1.0 - bound_ref[0]

    def step(b, carry):
        state, before = carry
        here = pl.ds(pl.multiple_of(b * BLOCK, BLOCK), BLOCK)
        weight = scale * jax.nn.sigmoid(-f_ref[here, :])
        log_forget = jnp.log1p(-weight)
        cumulative = dot_nn(lower, log_forget)
        queries = q_ref[here, :].astype(jnp.float32)
        values = v_ref[here, :].astype(jnp.float32)
        decayed_query = queries * jnp.exp(cumulative)
        decayed_key = weight * jnp.exp(-cumulative)
        scores = jnp.where(causal, dot_nt(decayed_query, decayed_key), 0.0)
        rec_ref[here, :] = dot_nt(decayed_query, state) + dot_nn(scores, values)
        query_ref[here, :] = queries * jnp.exp(cumulative + before)
        total = cumulative[BLOCK - 1 :, :]
        state = jnp.exp(total) * state + dot_tn(values, weight * jnp.exp(total - cumulative))
        return state, before + total

    state, total = lax.fori_loop(
        0,
        rows // BLOCK,
        step,
        (jnp.zeros((HEAD_DIM, HEAD_DIM), jnp.float32), jnp.zeros((1, HEAD_DIM), jnp.float32)),
    )
    state_ref[0] = state
    decay_ref[0] = jnp.broadcast_to(jnp.exp(total), decay_ref.shape[1:])


def recurrence(queries, forget_pre, value_in, lower_bound):
    rows, width = queries.shape
    heads = width // HEAD_DIM
    wide = pl.BlockSpec((rows, HEAD_DIM), lambda h: (0, h))
    return pl.pallas_call(
        recurrence_kernel,
        grid=(heads,),
        in_specs=[wide, wide, wide, pl.BlockSpec((1, 1, HEAD_DIM), lambda h: (h, 0, 0))],
        out_specs=[
            wide,
            wide,
            pl.BlockSpec((1, HEAD_DIM, HEAD_DIM), lambda h: (h, 0, 0)),
            pl.BlockSpec((1, 8, HEAD_DIM), lambda h: (h, 0, 0)),
        ],
        out_shape=[
            jax.ShapeDtypeStruct((rows, width), jnp.float32),
            jax.ShapeDtypeStruct((rows, width), jnp.float32),
            jax.ShapeDtypeStruct((heads, HEAD_DIM, HEAD_DIM), jnp.float32),
            jax.ShapeDtypeStruct((heads, 8, HEAD_DIM), jnp.float32),
        ],
        name="recurrence",
    )(queries, forget_pre, value_in, lower_bound.reshape(heads, 1, HEAD_DIM))


def prefix_kernel(pieces_ref, out_ref):
    def step(k, before):
        out_ref[k] = before
        return before * pieces_ref[k, 8:, :] + pieces_ref[k, :8, :]

    lax.fori_loop(0, pieces_ref.shape[0], step, jnp.zeros(out_ref.shape[1:], jnp.float32))


def prefix(pieces):
    return pl.pallas_call(
        prefix_kernel,
        out_shape=jax.ShapeDtypeStruct((pieces.shape[0], 8, HEAD_DIM), jnp.float32),
        name="prefix",
    )(pieces)


def gate_kernel(rec_ref, query_ref, state_ref, out_gate_ref, gain_ref, out_ref):
    rec = rec_ref[...] + dot_nt(query_ref[...], state_ref[0])
    act = jax.nn.silu(out_gate_ref[...].astype(jnp.float32))
    out_ref[...] = (rms_scale(rec, gain_ref[...]) * act).astype(jnp.bfloat16)


def gate(rec, query, state, out_gate, out_gain):
    rows, width = rec.shape
    wide = pl.BlockSpec((rows, HEAD_DIM), lambda h: (0, h))
    return pl.pallas_call(
        gate_kernel,
        grid=(width // HEAD_DIM,),
        in_specs=[
            wide,
            wide,
            pl.BlockSpec((1, HEAD_DIM, HEAD_DIM), lambda h: (h, 0, 0)),
            wide,
            pl.BlockSpec((1, HEAD_DIM), lambda h: (0, 0)),
        ],
        out_specs=wide,
        out_shape=jax.ShapeDtypeStruct((rows, width), jnp.bfloat16),
        name="gate",
    )(rec, query, state, out_gate, out_gain.reshape(1, HEAD_DIM))


def mixer(queries, forget_pre, value_in, out_gate, lower_bound, out_gain, out_weight):
    heads = queries.shape[1] // HEAD_DIM
    spans = lax.axis_size(EP)
    lanes = lax.axis_size("tp")
    rec, query, state, decay = recurrence(queries, forget_pre, value_in, lower_bound)
    per_head = spans // heads
    decays = jnp.broadcast_to(decay[:, None], (heads, per_head, 8, HEAD_DIM))
    leaving = jnp.concatenate(
        [
            state.reshape(spans, heads * HEAD_DIM // spans, HEAD_DIM),
            decays.reshape(spans, 8, HEAD_DIM),
        ],
        axis=1,
    )
    pieces = lax.all_to_all(leaving, EP, split_axis=0, concat_axis=0, tiled=True)
    before = prefix(pieces)
    starts = lax.all_to_all(before, EP, split_axis=0, concat_axis=0, tiled=True)
    gated = gate(rec, query, starts.reshape(heads, HEAD_DIM, HEAD_DIM), out_gate, out_gain)
    parts = jnp.dot(gated, out_weight, preferred_element_type=jnp.float32).astype(jnp.bfloat16)
    lane = lax.axis_index("tp")
    share = parts.shape[0] // lanes
    total = None
    for by in range(lanes):
        part = lax.dynamic_slice_in_dim(parts, (lane + by) % lanes * share, share, 0)
        if by > 0:
            part = lax.ppermute(part, "tp", [(i, (i + by) % lanes) for i in range(lanes)])
        part = part.astype(jnp.float32)
        total = part if total is None else total + part
    return total.astype(jnp.bfloat16)


def expert_kernel(core_ref, *refs):
    sets, steps = 1, 4
    row_refs = refs[:sets]
    sources = refs[sets : sets + 4 * steps]
    out_refs = refs[sets + 4 * steps : 2 * sets + 4 * steps]
    in_buffer, out_buffer, sum_ref, sems = refs[2 * sets + 4 * steps :]
    rows = row_refs[0].shape[0]
    half = out_buffer.shape[2]

    def copy(step, kind):
        buffer = in_buffer if kind < 2 else out_buffer
        place = 2 * step + kind % 2
        return pltpu.make_async_copy(
            sources[kind * steps + step], buffer.at[place], sems.at[4 * step + kind]
        )

    for step in range(steps):
        for kind in range(4):
            copy(step, kind).start()
    gate_is_own = core_ref[0] == 0
    for step in range(steps):
        for kind in range(4):
            copy(step, kind).wait()
        for s in range(sets):
            here = slice(s * rows, (s + 1) * rows)
            own = dot_nn(row_refs[s][...], in_buffer[2 * step], None)
            other = dot_nn(row_refs[s][...], in_buffer[2 * step + 1], None)
            gate_pre = jnp.where(gate_is_own, own, other)
            up_pre = jnp.where(gate_is_own, other, own)
            hidden = (jax.nn.silu(gate_pre) * up_pre).astype(jnp.bfloat16)
            for side in range(2):
                part = dot_nn(hidden, out_buffer[2 * step + side], None)
                if step > 0:
                    part = part + sum_ref[side, here, :]
                sum_ref[side, here, :] = part
    for s in range(sets):
        here = slice(s * rows, (s + 1) * rows)
        for side in range(2):
            place = (core_ref[0] if side == 0 else 1 - core_ref[0]) * half
            out_refs[s][:, pl.ds(pl.multiple_of(place, half), half)] = sum_ref[
                side, here, :
            ].astype(jnp.bfloat16)


def expert_rows(core, row_set, own_in, other_in, own_out, other_out):
    rows, width = row_set.shape
    units = own_in[0].shape[1]
    half = own_out[0].shape[1]
    vmem = pl.BlockSpec(memory_space=pltpu.VMEM)
    hbm = pl.BlockSpec(memory_space=pl.ANY)
    return pl.pallas_call(
        expert_kernel,
        in_specs=[pl.BlockSpec(memory_space=pltpu.SMEM), vmem] + [hbm] * 16,
        out_specs=vmem,
        out_shape=jax.ShapeDtypeStruct((rows, width), jnp.bfloat16),
        scratch_shapes=[
            pltpu.VMEM((8, width, units), jnp.bfloat16),
            pltpu.VMEM((8, units, half), jnp.bfloat16),
            pltpu.VMEM((2, rows, half), jnp.float32),
            pltpu.SemaphoreType.DMA((16,)),
        ],
        cost_estimate=pl.CostEstimate(
            flops=6 * rows * width * 1024, bytes_accessed=16 * 2**20, transcendentals=0
        ),
        name="expert_rows",
    )(core, row_set, *own_in, *other_in, *own_out, *other_out)


def slot_places(slot_count):
    slot = jnp.arange(slot_count, dtype=jnp.int32)
    device, place = slot // 2, slot % 2
    expert = device // 8 * 4 + device % 4
    return expert, device // 4 % 2 * 2 + place


def slots_filled(ids, slot_count):
    expert, rank = slot_places(slot_count)
    named = jnp.any(ids.T[:, None, :] == expert[None, :, None], axis=0)
    order = jnp.arange(ids.shape[0], dtype=jnp.int32)
    earlier = (order[:, None] < order[None, :]).astype(jnp.bfloat16)
    ranks = jnp.dot(named.astype(jnp.bfloat16), earlier, preferred_element_type=jnp.float32)
    return named & (ranks == rank.astype(jnp.float32)[:, None])


def slot_weights(ids, weights, slot_count):
    expert, rank = slot_places(slot_count)
    named = ids[:, :, None] == expert[None, None, :]
    weight = jnp.sum(jnp.where(named, weights[:, :, None], 0.0), axis=1)
    named = jnp.any(named, axis=1)
    order = jnp.arange(ids.shape[0], dtype=jnp.int32)
    earlier = (order[None, :] < order[:, None]).astype(jnp.bfloat16)
    ranks = jnp.dot(earlier, named.astype(jnp.bfloat16), preferred_element_type=jnp.float32)
    return jnp.where(ranks == rank.astype(jnp.float32)[None, :], weight, 0.0)


def weight_moves(turn):
    moves = []
    for core in range(2):
        for lane in range(4):
            piece = lane ^ turn
            moves.append((core * 4 + lane, (piece % 2) * 4 + 2 * core + piece // 2))
    return moves


RING = ("ep_2", "tp")


def experts(moe_tokens, moe_gain, expert_ids, route_weights, w_gate, w_up, w_down):
    lanes = lax.axis_size("tp")
    lane = lax.axis_index("tp")
    core = lax.axis_index("ep_2")
    devices = lax.axis_size(EP_TP)
    model_width = w_gate.shape[1]
    qrows = moe_tokens.shape[0] // lanes
    slots = 2 * devices
    half = model_width // 2

    own_in, own_out, other_in, other_out = [], [], [], []
    for turn in range(4):
        piece = lane ^ turn
        expert, part = piece // 2, piece % 2
        gate_now = lax.dynamic_index_in_dim(w_gate, expert, 0, keepdims=False)
        up_now = lax.dynamic_index_in_dim(w_up, expert, 0, keepdims=False)
        in_now = jnp.where(part == 0, gate_now, up_now)
        down_now = lax.dynamic_slice(
            w_down, (expert, 0, part * half), (1, w_down.shape[1], half)
        )[0]
        own_in.append(lax.ppermute(in_now, RING, weight_moves(turn)))
        own_out.append(lax.ppermute(down_now, RING, weight_moves(turn)))
    for turn in range(4):
        other_in.append(lax.ppermute(own_in[turn ^ 1], "ep_2", [(0, 1), (1, 0)]))
        other_out.append(lax.ppermute(own_out[turn ^ 1], "ep_2", [(0, 1), (1, 0)]))

    start = lane * qrows
    ids = lax.dynamic_slice_in_dim(expert_ids, start, qrows, 0)
    weights = lax.dynamic_slice_in_dim(route_weights, start, qrows, 0)
    tokens = lax.dynamic_slice_in_dim(moe_tokens, start, qrows, 0)
    normed = rms_scale(tokens.astype(jnp.float32), moe_gain).astype(jnp.bfloat16)
    filled = slots_filled(ids, slots).astype(jnp.bfloat16)
    leaving = jnp.dot(filled, normed, preferred_element_type=jnp.float32).astype(jnp.bfloat16)
    arrived = lax.all_to_all(
        leaving.reshape(devices, 2, model_width), EP_TP, 0, 0, tiled=True
    )

    results = expert_rows(
        core.astype(jnp.int32).reshape(1),
        arrived.reshape(slots, model_width),
        own_in,
        other_in,
        own_out,
        other_out,
    )

    returned = lax.all_to_all(
        results.reshape(devices, 2, model_width), EP_TP, 0, 0, tiled=True
    )
    returned = returned.reshape(slots, model_width)
    mix = slot_weights(ids, weights, slots)
    high = lax.reduce_precision(mix, 8, 7)
    out = jnp.dot(high.astype(jnp.bfloat16), returned, preferred_element_type=jnp.float32)
    out += jnp.dot(
        (mix - high).astype(jnp.bfloat16), returned, preferred_element_type=jnp.float32
    )
    return out.astype(jnp.bfloat16)


def local(
    queries,
    forget_pre,
    value_in,
    out_gate,
    lower_bound,
    out_gain,
    out_weight,
    moe_tokens,
    moe_gain,
    expert_ids,
    route_weights,
    w_gate,
    w_up,
    w_down,
):
    expert_out = experts(
        moe_tokens, moe_gain, expert_ids, route_weights, w_gate, w_up, w_down
    )
    mixer_out = mixer(queries, forget_pre, value_in, out_gate, lower_bound, out_gain, out_weight)
    return mixer_out, expert_out


def solution(mesh):
    split = Mesh(mesh.devices.reshape(8, 4, 2, mesh.shape["tp"]), ("ep_0", "ep_1", "ep_2", "tp"))
    placed = (
        P(EP, "tp"),
        P(EP, "tp"),
        P(EP, "tp"),
        P(EP, "tp"),
        P("tp"),
        P(),
        P("tp", None),
        P(EP, None),
        P(),
        P(EP, None),
        P(EP, None),
        P(EP, None, "tp"),
        P(EP, None, "tp"),
        P(EP, "tp", None),
    )
    return jax.shard_map(
        local,
        mesh=split,
        in_specs=placed,
        out_specs=(P(EP_TP, None), P(EP_TP, None)),
        check_vma=False,
    )
```

profile of v0, /device:TPU:8, one launch (start us, length us, event | category | flops | bytes accessed | tf_op | source)
XLA Modules:
  0.0 278.4 jit_solution(3722979773385229297)
XLA Ops:
  0.7 26.4 %recurrence.1 = (f32[512,512]{1,0:T(8,128)}, f32[512,512]{1,0:T(8,128)}, f32[4,128,128]{2,1,0:T(8,128)}, f32[4,8,128]{2,1,0:T(8,128)}) custom-call(bf16[512,512]{1,0:T(8,128)(2,1)} %q_ref.1, f32[512,512]{1,0:T(8,128)} %f_ref.1, bf16[512,512]{1,0:T(8,128)(2,1)} %v_ref.1, f32[4,1,128]{2,1,0:T(1,128)} %bitcast.33), custom_call_target="tpu_custom_call" | custom-call | tf_op jit(solution)/shard_map/recurrence/pallas_call | solution.py:80
  27.8 1.8 pad_maximum_fusion
  29.7 12.1 %all-to-all-start = ((f32[64,16,128]{2,1,0:T(8,128)}), f32[64,16,128]{2,1,0:T(8,128)S(1)}, u32[]{:S(2)}, u32[]{:S(2)}) async-start(f32[64,16,128]{2,1,0:T(8,128)} %pad_maximum_fusion), calls=%async_computation | async-start | bytes 1048576 | tf_op jit(solution)/shard_map/all_to_all | solution.py:155
  43.1 3.3 %convolution_convert_fusion = bf16[512,2048]{1,0:T(8,128)(2,1)} fusion(pred[512,64]{0,1:T(8,128)(4,1)S(1)} %compare_reduce_fusion.1, f32[2048]{0:T(1024)S(1)} %copy-done.5, f32[64]{0:T(128)S(1)} %add_rsqrt_fusion, bf16[256,2048]{1,0:T(8,128)(2,1)} %param.21, s32[]{:T(128)S(6)} %select_n.258, f32[512]{0:T(512)S(1)} %get-tuple-element.22), kind=kOutput, calls=%fused_computation | convolution fusion | flops 140054528 | bytes 2435588 | tf_op jit(solution)/shard_map/dot_general | solution.py:311
  46.4 4.4 %reshape.241 = bf16[256,2,2048]{2,1,0:T(2,128)(2,1)} reshape(bf16[512,2048]{1,0:T(8,128)(2,1)} %convolution_convert_fusion) | data formatting | bytes 4194304 | tf_op jit(solution)/shard_map/reshape | solution.py:313
  50.8 8.5 %all-to-all-done.pieces_ref = f32[64,16,128]{2,1,0:T(8,128)S(1)} async-done(((f32[64,16,128]{2,1,0:T(8,128)}), f32[64,16,128]{2,1,0:T(8,128)S(1)}, u32[]{:S(2)}, u32[]{:S(2)}) %all-to-all-start) | async-done | bytes 524320 | tf_op jit(solution)/shard_map/all_to_all | solution.py:155
  59.3 9.4 %all-to-all-start.2 = ((bf16[256,2,2048]{2,1,0:T(2,128)(2,1)}), bf16[256,2,2048]{2,1,0:T(2,128)(2,1)}, u32[]{:S(2)}, u32[]{:S(2)}) async-start(bf16[256,2,2048]{2,1,0:T(2,128)(2,1)} %reshape.241), calls=%async_computation.2 | async-start | bytes 4194304 | tf_op jit(solution)/shard_map/all_to_all | solution.py:312
  68.8 2.8 %dynamic-slice_bitcast_fusion = (bf16[256,1024]{1,0:T(8,128)(2,1)S(1)}, bf16[256,1024]{1,0:T(8,128)(2,1)}, bf16[256,1024]{1,0:T(8,128)(2,1)}, bf16[256,1024]{1,0:T(8,128)(2,1)S(1)}) fusion(bf16[2,256,2048]{2,1,0:T(8,128)(2,1)} %param.27, s32[]{:T(128)S(6)} %select_n.288, s32[]{:T(128)S(6)} %select_n.294, s32[]{:T(128)S(6)} %select_n.276, s32[]{:T(128)S(6)} %select_n.292, ...), kind=kLoop, calls=%fused_computation.22 | loop fusion | bytes 4194336 | tf_op jit(solution)/shard_map/squeeze | solution.py:296
  71.7 5.4 %collective-permute-start.11 = (bf16[256,1024]{1,0:T(8,128)(2,1)}, bf16[256,1024]{1,0:T(8,128)(2,1)}, u32[]{:S(2)}, u32[]{:S(2)}) collective-permute-start(bf16[256,1024]{1,0:T(8,128)(2,1)} %get-tuple-element.16), channel_id=1, source_target_pairs={{0,0},{1,4},{2,1},{3,5},{4,2},{5,6},{6,3},{7,7},{8,8},{9,12},{10,9... | collective-permute-start | bytes 1572872 | tf_op jit(solution)/shard_map/ppermute | solution.py:300
  77.1 1.9 collective-permute-start.14
  79.0 3.8 %select_bitcast_fusion = (bf16[2048,256]{1,0:T(8,128)(2,1)S(1)}, bf16[2048,256]{1,0:T(8,128)(2,1)S(1)}, bf16[2048,256]{1,0:T(8,128)(2,1)S(1)}, bf16[2048,256]{1,0:T(8,128)(2,1)S(1)}) fusion(bf16[2,2048,256]{2,1,0:T(8,128)(2,1)} %param.26, s32[]{:T(128)S(6)} %select_n.288, bf16[2,2048,256]{2,1,0:T(8,128)(2,1)} %param.25, pred[]{:T(512)S(6)} %eq.83, ...), kind=kLoop, calls=%fused_computation.8 | loop fusion | flops 2097152 | bytes 12582932 | tf_op jit(solution)/shard_map/jit(_where)/select_n | solution.py:295
  83.3 3.0 %collective-permute-start.4 = (bf16[2048,256]{1,0:T(8,128)(2,1)S(1)}, bf16[2048,256]{1,0:T(8,128)(2,1)}, u32[]{:S(2)}, u32[]{:S(2)}) collective-permute-start(bf16[2048,256]{1,0:T(8,128)(2,1)S(1)} %get-tuple-element.11), channel_id=1, source_target_pairs={{0,4},{1,0},{2,5},{3,1},{4,6},{5,2},{6,7},{7,3},{8,12},{9,8},{10,1... | collective-permute-start | bytes 3145736 | tf_op jit(solution)/shard_map/ppermute | solution.py:299
  87.7 1.7 collective-permute-start.3
  89.3 30.0 %collective-permute-start.6 = (bf16[2048,256]{1,0:T(8,128)(2,1)S(1)}, bf16[2048,256]{1,0:T(8,128)(2,1)}, u32[]{:S(2)}, u32[]{:S(2)}) collective-permute-start(bf16[2048,256]{1,0:T(8,128)(2,1)S(1)} %get-tuple-element.10), channel_id=1, source_target_pairs={{0,5},{1,1},{2,4},{3,0},{4,7},{5,3},{6,6},{7,2},{8,13},{9,9},{10,1... | collective-permute-start | bytes 3145736 | tf_op jit(solution)/shard_map/ppermute | solution.py:299
  119.3 1.5 collective-permute-start.13
  120.8 41.1 %collective-permute-done.13.refs_11_ = bf16[256,1024]{1,0:T(8,128)(2,1)S(1)} collective-permute-done((bf16[256,1024]{1,0:T(8,128)(2,1)S(1)}, bf16[256,1024]{1,0:T(8,128)(2,1)S(1)}, u32[]{:S(2)}, u32[]{:S(2)}) %collective-permute-start.13) | collective-permute-done | bytes 524320 | tf_op jit(solution)/shard_map/ppermute | solution.py:300
  161.9 4.1 %collective-permute-start.15 = (bf16[256,1024]{1,0:T(8,128)(2,1)}, bf16[256,1024]{1,0:T(8,128)(2,1)S(1)}, u32[]{:S(2)}, u32[]{:S(2)}) collective-permute-start(bf16[256,1024]{1,0:T(8,128)(2,1)} %collective-permute-done.12.refs_10_), channel_id=1, source_target_pairs={{0,4},{4,0},{1,5},{5,1},{2,6},{6,2},{3,7},{7,3},{8,12},{12,8},{9,1... | collective-permute-start | bytes 1572872 | tf_op jit(solution)/shard_map/ppermute | solution.py:303
  170.5 2.1 prefix.1
  172.6 9.3 %all-to-all-start.1 = ((f32[64,8,128]{2,1,0:T(8,128)}), f32[64,8,128]{2,1,0:T(8,128)S(1)}, u32[]{:S(2)}, u32[]{:S(2)}) async-start(f32[64,8,128]{2,1,0:T(8,128)} %prefix.1), calls=%async_computation.1 | async-start | bytes 524288 | tf_op jit(solution)/shard_map/all_to_all | solution.py:157
  182.0 4.1 %reshape.242.refs_0_ = bf16[512,2048]{1,0:T(8,128)(2,1)} reshape(bf16[256,2,2048]{2,1,0:T(2,128)(2,1)} %all-to-all-done.2) | data formatting | bytes 4194304 | tf_op jit(solution)/shard_map/reshape | solution.py:318
  186.1 12.1 %expert_rows.1 = bf16[512,2048]{1,0:T(8,128)(2,1)} custom-call(s32[1]{0:T(128)} %bitcast.5.core_ref, bf16[512,2048]{1,0:T(8,128)(2,1)} %reshape.242.refs_0_, bf16[2048,256]{1,0:T(8,128)(2,1)} %collective-permute-done.3.refs_1_, bf16[2048,256]{1,0:T(8,128)(2,1)} %collective-permute-done.4.refs_2_, bf16[2048,256]{1,0:T(8,128)(2,1)} %collective-permute-done.5.refs_3_, ...), custom_call_target="tpu_custom_call" | custom-call | flops 6442450944 | bytes 16777216 | tf_op jit(solution)/shard_map/expert_rows/pallas_call | solution.py:222
  198.3 4.4 %reshape.243 = bf16[256,2,2048]{2,1,0:T(2,128)(2,1)} reshape(bf16[512,2048]{1,0:T(8,128)(2,1)} %expert_rows.1) | data formatting | bytes 4194304 | tf_op jit(solution)/shard_map/reshape | solution.py:326
  203.4 12.6 %all-to-all-start.3 = ((bf16[256,2,2048]{2,1,0:T(2,128)(2,1)}), bf16[256,2,2048]{2,1,0:T(2,128)(2,1)}, u32[]{:S(2)}, u32[]{:S(2)}) async-start(bf16[256,2,2048]{2,1,0:T(2,128)(2,1)} %reshape.243), calls=%async_computation.3 | async-start | bytes 4194304 | tf_op jit(solution)/shard_map/all_to_all | solution.py:325
  216.1 4.5 %gate.1 = bf16[512,512]{1,0:T(8,128)(2,1)} custom-call(f32[512,512]{1,0:T(8,128)} %get-tuple-element.6.rec_ref, f32[512,512]{1,0:T(8,128)} %get-tuple-element.7.query_ref, f32[4,128,128]{2,1,0:T(8,128)} %bitcast.30, bf16[512,512]{1,0:T(8,128)(2,1)} %out_gate_ref.1, f32[1,128]{1,0:T(1,128)} %bitcast.34), custom_call_target="tpu_custom_call" | custom-call | tf_op jit(solution)/shard_map/gate/pallas_call | solution.py:125
  220.6 2.3 convolution_convert_fusion.1
  225.2 1.5 collective-permute-start
  226.7 2.7 collective-permute-start.1
  231.3 17.4 %collective-permute-done = bf16[128,2048]{1,0:T(8,128)(2,1)} collective-permute-done((bf16[128,2048]{1,0:T(8,128)(2,1)}, bf16[128,2048]{1,0:T(8,128)(2,1)}, u32[]{:S(2)}, u32[]{:S(2)}) %collective-permute-start) | collective-permute-done | bytes 524320 | tf_op jit(solution)/shard_map/ppermute | solution.py:166
  248.7 19.5 %collective-permute-done.1 = bf16[128,2048]{1,0:T(8,128)(2,1)} collective-permute-done((bf16[128,2048]{1,0:T(8,128)(2,1)S(1)}, bf16[128,2048]{1,0:T(8,128)(2,1)}, u32[]{:S(2)}, u32[]{:S(2)}) %collective-permute-start.1) | collective-permute-done | bytes 524320 | tf_op jit(solution)/shard_map/ppermute | solution.py:166
  268.3 2.6 add_convert_fusion
  270.9 4.1 %reshape.244 = bf16[512,2048]{1,0:T(8,128)(2,1)} reshape(bf16[256,2,2048]{2,1,0:T(2,128)(2,1)} %all-to-all-done.3) | data formatting | bytes 4194304 | tf_op jit(solution)/shard_map/reshape | solution.py:328
  275.0 2.2 fusion.12
  (66 shorter events, 14.8 us)
Async XLA Ops:
  0.6 220.0 %copy-start = (bf16[512,2048]{1,0:T(8,128)(2,1)S(1)}, bf16[512,2048]{1,0:T(8,128)(2,1)}, u32[]{:S(2)}) copy-start(bf16[512,2048]{1,0:T(8,128)(2,1)} %param.20) | copy-start | bytes 6291460
  0.6 42.2 %copy-start.6 = (s32[256,4]{0,1:T(4,128)S(1)}, s32[256,4]{0,1:T(4,128)}, u32[]{:S(2)}) copy-start(s32[256,4]{0,1:T(4,128)} %param.23) | copy-start | bytes 12292
  0.7 42.5 %copy-start.5 = (f32[2048]{0:T(1024)S(1)}, f32[2048]{0:T(1024)}, u32[]{:S(2)}) copy-start(f32[2048]{0:T(1024)} %param.22) | copy-start | bytes 24580
  29.7 29.6 %all-to-all-start = ((f32[64,16,128]{2,1,0:T(8,128)}), f32[64,16,128]{2,1,0:T(8,128)S(1)}, u32[]{:S(2)}, u32[]{:S(2)}) async-start(f32[64,16,128]{2,1,0:T(8,128)} %pad_maximum_fusion), calls=%async_computation | async-start | bytes 1048576 | tf_op jit(solution)/shard_map/all_to_all | solution.py:155
  59.3 9.4 %copy-start.3 = (f32[64,16,128]{2,1,0:T(8,128)}, f32[64,16,128]{2,1,0:T(8,128)S(1)}, u32[]{:S(2)}) copy-start(f32[64,16,128]{2,1,0:T(8,128)S(1)} %all-to-all-done.pieces_ref) | copy-start | bytes 1572868
  59.3 113.3 %all-to-all-start.2 = ((bf16[256,2,2048]{2,1,0:T(2,128)(2,1)}), bf16[256,2,2048]{2,1,0:T(2,128)(2,1)}, u32[]{:S(2)}, u32[]{:S(2)}) async-start(bf16[256,2,2048]{2,1,0:T(2,128)(2,1)} %reshape.241), calls=%async_computation.2 | async-start | bytes 4194304 | tf_op jit(solution)/shard_map/all_to_all | solution.py:312
  71.6 16.1 %collective-permute-start.12 = (bf16[256,1024]{1,0:T(8,128)(2,1)}, bf16[256,1024]{1,0:T(8,128)(2,1)}, u32[]{:S(2)}, u32[]{:S(2)}) collective-permute-start(bf16[256,1024]{1,0:T(8,128)(2,1)} %get-tuple-element.15), channel_id=1, source_target_pairs={{0,4},{1,0},{2,5},{3,1},{4,6},{5,2},{6,7},{7,3},{8,12},{9,8},{10,1... | collective-permute-start | bytes 1572872 | tf_op jit(solution)/shard_map/ppermute | solution.py:300
  71.7 17.6 %collective-permute-start.11 = (bf16[256,1024]{1,0:T(8,128)(2,1)}, bf16[256,1024]{1,0:T(8,128)(2,1)}, u32[]{:S(2)}, u32[]{:S(2)}) collective-permute-start(bf16[256,1024]{1,0:T(8,128)(2,1)} %get-tuple-element.16), channel_id=1, source_target_pairs={{0,0},{1,4},{2,1},{3,5},{4,2},{5,6},{6,3},{7,7},{8,8},{9,12},{10,9... | collective-permute-start | bytes 1572872 | tf_op jit(solution)/shard_map/ppermute | solution.py:300
  77.1 42.2 %collective-permute-start.14 = (bf16[256,1024]{1,0:T(8,128)(2,1)S(1)}, bf16[256,1024]{1,0:T(8,128)(2,1)}, u32[]{:S(2)}, u32[]{:S(2)}) collective-permute-start(bf16[256,1024]{1,0:T(8,128)(2,1)S(1)} %get-tuple-element.14), channel_id=1, source_target_pairs={{0,5},{1,1},{2,4},{3,0},{4,7},{5,3},{6,6},{7,2},{8,13},{9,9},{10,1... | collective-permute-start | bytes 1572872 | tf_op jit(solution)/shard_map/ppermute | solution.py:300
  82.9 83.1 %collective-permute-start.5 = (bf16[2048,256]{1,0:T(8,128)(2,1)S(1)}, bf16[2048,256]{1,0:T(8,128)(2,1)}, u32[]{:S(2)}, u32[]{:S(2)}) collective-permute-start(bf16[2048,256]{1,0:T(8,128)(2,1)S(1)} %get-tuple-element.13), channel_id=1, source_target_pairs={{0,1},{1,5},{2,0},{3,4},{4,3},{5,7},{6,2},{7,6},{8,9},{9,13},{10,8... | collective-permute-start | bytes 3145736 | tf_op jit(solution)/shard_map/ppermute | solution.py:299
  83.3 82.8 %collective-permute-start.4 = (bf16[2048,256]{1,0:T(8,128)(2,1)S(1)}, bf16[2048,256]{1,0:T(8,128)(2,1)}, u32[]{:S(2)}, u32[]{:S(2)}) collective-permute-start(bf16[2048,256]{1,0:T(8,128)(2,1)S(1)} %get-tuple-element.11), channel_id=1, source_target_pairs={{0,4},{1,0},{2,5},{3,1},{4,6},{5,2},{6,7},{7,3},{8,12},{9,8},{10,1... | collective-permute-start | bytes 3145736 | tf_op jit(solution)/shard_map/ppermute | solution.py:299
  87.7 78.8 %collective-permute-start.3 = (bf16[2048,256]{1,0:T(8,128)(2,1)S(1)}, bf16[2048,256]{1,0:T(8,128)(2,1)}, u32[]{:S(2)}, u32[]{:S(2)}) collective-permute-start(bf16[2048,256]{1,0:T(8,128)(2,1)S(1)} %get-tuple-element.12), channel_id=1, source_target_pairs={{0,0},{1,4},{2,1},{3,5},{4,2},{5,6},{6,3},{7,7},{8,8},{9,12},{10,9... | collective-permute-start | bytes 3145736 | tf_op jit(solution)/shard_map/ppermute | solution.py:299
  89.3 77.2 %collective-permute-start.6 = (bf16[2048,256]{1,0:T(8,128)(2,1)S(1)}, bf16[2048,256]{1,0:T(8,128)(2,1)}, u32[]{:S(2)}, u32[]{:S(2)}) collective-permute-start(bf16[2048,256]{1,0:T(8,128)(2,1)S(1)} %get-tuple-element.10), channel_id=1, source_target_pairs={{0,5},{1,1},{2,4},{3,0},{4,7},{5,3},{6,6},{7,2},{8,13},{9,9},{10,1... | collective-permute-start | bytes 3145736 | tf_op jit(solution)/shard_map/ppermute | solution.py:299
  119.3 42.5 %collective-permute-start.13 = (bf16[256,1024]{1,0:T(8,128)(2,1)S(1)}, bf16[256,1024]{1,0:T(8,128)(2,1)S(1)}, u32[]{:S(2)}, u32[]{:S(2)}) collective-permute-start(bf16[256,1024]{1,0:T(8,128)(2,1)S(1)} %get-tuple-element.17), channel_id=1, source_target_pairs={{0,1},{1,5},{2,0},{3,4},{4,3},{5,7},{6,2},{7,6},{8,9},{9,13},{10,8... | collective-permute-start | bytes 1572872 | tf_op jit(solution)/shard_map/ppermute | solution.py:300
  161.9 24.2 %copy-start.8 = (bf16[256,1024]{1,0:T(8,128)(2,1)}, bf16[256,1024]{1,0:T(8,128)(2,1)S(1)}, u32[]{:S(2)}) copy-start(bf16[256,1024]{1,0:T(8,128)(2,1)S(1)} %collective-permute-done.13.refs_11_) | copy-start | bytes 1572868
  161.9 5.9 %collective-permute-start.15 = (bf16[256,1024]{1,0:T(8,128)(2,1)}, bf16[256,1024]{1,0:T(8,128)(2,1)S(1)}, u32[]{:S(2)}, u32[]{:S(2)}) collective-permute-start(bf16[256,1024]{1,0:T(8,128)(2,1)} %collective-permute-done.12.refs_10_), channel_id=1, source_target_pairs={{0,4},{4,0},{1,5},{5,1},{2,6},{6,2},{3,7},{7,3},{8,12},{12,8},{9,1... | collective-permute-start | bytes 1572872 | tf_op jit(solution)/shard_map/ppermute | solution.py:303
  166.0 2.5 collective-permute-start.16
  166.1 3.1 %collective-permute-start.17 = (bf16[256,1024]{1,0:T(8,128)(2,1)}, bf16[256,1024]{1,0:T(8,128)(2,1)S(1)}, u32[]{:S(2)}, u32[]{:S(2)}) collective-permute-start(bf16[256,1024]{1,0:T(8,128)(2,1)} %collective-permute-done.14.refs_12_), channel_id=1, source_target_pairs={{0,4},{4,0},{1,5},{5,1},{2,6},{6,2},{3,7},{7,3},{8,12},{12,8},{9,1... | collective-permute-start | bytes 1572872 | tf_op jit(solution)/shard_map/ppermute | solution.py:303
  166.5 19.6 %collective-permute-start.10 = (bf16[2048,256]{1,0:T(8,128)(2,1)}, bf16[2048,256]{1,0:T(8,128)(2,1)}, u32[]{:S(2)}, u32[]{:S(2)}) collective-permute-start(bf16[2048,256]{1,0:T(8,128)(2,1)} %collective-permute-done.5.refs_3_), channel_id=1, source_target_pairs={{0,4},{4,0},{1,5},{5,1},{2,6},{6,2},{3,7},{7,3},{8,12},{12,8},{9,1... | collective-permute-start | bytes 3145736 | tf_op jit(solution)/shard_map/ppermute | solution.py:302
  166.6 19.5 %collective-permute-start.7 = (bf16[2048,256]{1,0:T(8,128)(2,1)}, bf16[2048,256]{1,0:T(8,128)(2,1)}, u32[]{:S(2)}, u32[]{:S(2)}) collective-permute-start(bf16[2048,256]{1,0:T(8,128)(2,1)} %collective-permute-done.4.refs_2_), channel_id=1, source_target_pairs={{0,4},{4,0},{1,5},{5,1},{2,6},{6,2},{3,7},{7,3},{8,12},{12,8},{9,1... | collective-permute-start | bytes 3145736 | tf_op jit(solution)/shard_map/ppermute | solution.py:302
  167.7 1.1 copy-start.9
  167.7 18.4 %collective-permute-start.8 = (bf16[2048,256]{1,0:T(8,128)(2,1)}, bf16[2048,256]{1,0:T(8,128)(2,1)}, u32[]{:S(2)}, u32[]{:S(2)}) collective-permute-start(bf16[2048,256]{1,0:T(8,128)(2,1)} %collective-permute-done.3.refs_1_), channel_id=1, source_target_pairs={{0,4},{4,0},{1,5},{5,1},{2,6},{6,2},{3,7},{7,3},{8,12},{12,8},{9,1... | collective-permute-start | bytes 3145736 | tf_op jit(solution)/shard_map/ppermute | solution.py:302
  168.5 17.7 %collective-permute-start.9 = (bf16[2048,256]{1,0:T(8,128)(2,1)}, bf16[2048,256]{1,0:T(8,128)(2,1)}, u32[]{:S(2)}, u32[]{:S(2)}) collective-permute-start(bf16[2048,256]{1,0:T(8,128)(2,1)} %collective-permute-done.6.refs_4_), channel_id=1, source_target_pairs={{0,4},{4,0},{1,5},{5,1},{2,6},{6,2},{3,7},{7,3},{8,12},{12,8},{9,1... | collective-permute-start | bytes 3145736 | tf_op jit(solution)/shard_map/ppermute | solution.py:302
  170.1 16.0 %collective-permute-start.18 = (bf16[256,1024]{1,0:T(8,128)(2,1)S(1)}, bf16[256,1024]{1,0:T(8,128)(2,1)}, u32[]{:S(2)}, u32[]{:S(2)}) collective-permute-start(bf16[256,1024]{1,0:T(8,128)(2,1)S(1)} %collective-permute-done.13.refs_11_), channel_id=1, source_target_pairs={{0,4},{4,0},{1,5},{5,1},{2,6},{6,2},{3,7},{7,3},{8,12},{12,8},{9,1... | collective-permute-start | bytes 1572872 | tf_op jit(solution)/shard_map/ppermute | solution.py:303
  172.6 30.0 %all-to-all-start.1 = ((f32[64,8,128]{2,1,0:T(8,128)}), f32[64,8,128]{2,1,0:T(8,128)S(1)}, u32[]{:S(2)}, u32[]{:S(2)}) async-start(f32[64,8,128]{2,1,0:T(8,128)} %prefix.1), calls=%async_computation.1 | async-start | bytes 524288 | tf_op jit(solution)/shard_map/all_to_all | solution.py:157
  203.4 67.5 %all-to-all-start.3 = ((bf16[256,2,2048]{2,1,0:T(2,128)(2,1)}), bf16[256,2,2048]{2,1,0:T(2,128)(2,1)}, u32[]{:S(2)}, u32[]{:S(2)}) async-start(bf16[256,2,2048]{2,1,0:T(2,128)(2,1)} %reshape.243), calls=%async_computation.3 | async-start | bytes 4194304 | tf_op jit(solution)/shard_map/all_to_all | solution.py:325
  222.9 1.4 copy-start.2
  224.3 6.5 %copy-start.7 = (f32[256,4]{0,1:T(4,128)S(1)}, f32[256,4]{0,1:T(4,128)}, u32[]{:S(2)}) copy-start(f32[256,4]{0,1:T(4,128)} %param.24) | copy-start | bytes 12292
  225.2 23.5 %collective-permute-start = (bf16[128,2048]{1,0:T(8,128)(2,1)}, bf16[128,2048]{1,0:T(8,128)(2,1)}, u32[]{:S(2)}, u32[]{:S(2)}) collective-permute-start(bf16[128,2048]{1,0:T(8,128)(2,1)} %get-tuple-element.18), channel_id=1, source_target_pairs={{0,1},{1,2},{2,3},{3,0},{4,5},{5,6},{6,7},{7,4},{8,9},{9,10},{10,1... | collective-permute-start | bytes 1572872 | tf_op jit(solution)/shard_map/ppermute | solution.py:166
  226.7 41.6 %collective-permute-start.1 = (bf16[128,2048]{1,0:T(8,128)(2,1)S(1)}, bf16[128,2048]{1,0:T(8,128)(2,1)}, u32[]{:S(2)}, u32[]{:S(2)}) collective-permute-start(bf16[128,2048]{1,0:T(8,128)(2,1)S(1)} %get-tuple-element.20), channel_id=1, source_target_pairs={{0,2},{1,3},{2,0},{3,1},{4,6},{5,7},{6,4},{7,5},{8,10},{9,11},{10,... | collective-permute-start | bytes 1572872 | tf_op jit(solution)/shard_map/ppermute | solution.py:166
  229.3 38.9 %collective-permute-start.2 = (bf16[128,2048]{1,0:T(8,128)(2,1)S(1)}, bf16[128,2048]{1,0:T(8,128)(2,1)}, u32[]{:S(2)}, u32[]{:S(2)}) collective-permute-start(bf16[128,2048]{1,0:T(8,128)(2,1)S(1)} %get-tuple-element.19), channel_id=1, source_target_pairs={{0,3},{1,0},{2,1},{3,2},{4,7},{5,4},{6,5},{7,6},{8,11},{9,8},{10,9... | collective-permute-start | bytes 1572872 | tf_op jit(solution)/shard_map/ppermute | solution.py:166
  275.0 2.2 copy-start.1
  (3 other events, 2.3 us)
where the time goes:
time: 281 us; the launch traced here: 278 us
  starting transfers between devices  99.2 us (35%)
  waiting for transfers between devices  89.4 us (32%)
  Pallas kernels  45.2 us (16%)
  local copies, waits for them, and re-layouts  24.7 us (9%)
  other arithmetic  9.83 us (3%)
  matrix products  9.13 us (3%)
    ppermute x4, waiting for transfers between devices, experts(): own_out.append(lax.ppermute(down_now, RING, weight_moves(turn)))  42.4 us
    ppermute x3, waiting for transfers between devices, mixer(): lax.ppermute(part, 'tp', [(i, (i + by) % lanes) for i in range(lanes)])  36.9 us
    ppermute x4, starting transfers between devices, experts(): own_in.append(lax.ppermute(in_now, RING, weight_moves(turn)))  35.1 us
    pallas_call x1, Pallas kernels, recurrence(): pl.pallas_call(recurrence_kernel, grid=(heads,), in_specs=[wide, wide, wi...  26.4 us
    all_to_all x1, starting transfers between devices, experts(): lax.all_to_all(results.reshape(devices, 2, model_width), EP_TP, 0, 0, til...  12.6 us
    pallas_call x1, Pallas kernels, expert_rows(): pl.pallas_call(expert_kernel, in_specs=[pl.BlockSpec(memory_space=pltpu.S...  12.1 us
    all_to_all x1, starting transfers between devices, mixer(): lax.all_to_all(leaving, EP, split_axis=0, concat_axis=0, tiled=True)  12.1 us
    all_to_all x1, starting transfers between devices, experts(): lax.all_to_all(leaving.reshape(devices, 2, model_width), EP_TP, 0, 0, til...  9.35 us
  transfers between devices with their start and end apart: 23, of which 8 were waited for; matrix products, arithmetic and copies ran while one was open for 11% of the time, Pallas kernels for 7%

commit v1 on v0

--- a/solution.py
+++ b/solution.py
@@ -169,72 +169,65 @@
     return total.astype(jnp.bfloat16)
 
 
-def expert_kernel(core_ref, *refs):
-    sets, steps = 1, 4
-    row_refs = refs[:sets]
-    sources = refs[sets : sets + 4 * steps]
-    out_refs = refs[sets + 4 * steps : 2 * sets + 4 * steps]
-    in_buffer, out_buffer, sum_ref, sems = refs[2 * sets + 4 * steps :]
-    rows = row_refs[0].shape[0]
-    half = out_buffer.shape[2]
-
-    def copy(step, kind):
-        buffer = in_buffer if kind < 2 else out_buffer
-        place = 2 * step + kind % 2
-        return pltpu.make_async_copy(
-            sources[kind * steps + step], buffer.at[place], sems.at[4 * step + kind]
-        )
-
-    for step in range(steps):
-        for kind in range(4):
-            copy(step, kind).start()
+STEPS = 4
+
+
+def expert_kernel(core_ref, row_ref, *refs):
+    sources = refs[: 2 * STEPS]
+    out_ref, weight_ref, sems = refs[2 * STEPS :]
+    width = row_ref.shape[1]
+    units = weight_ref.shape[2]
+    half = width // 2
+
+    def copy(place):
+        return pltpu.make_async_copy(sources[place], weight_ref.at[place], sems.at[place])
+
+    for place in range(2 * STEPS):
+        copy(place).start()
     gate_is_own = core_ref[0] == 0
-    for step in range(steps):
-        for kind in range(4):
-            copy(step, kind).wait()
-        for s in range(sets):
-            here = slice(s * rows, (s + 1) * rows)
-            own = dot_nn(row_refs[s][...], in_buffer[2 * step], None)
-            other = dot_nn(row_refs[s][...], in_buffer[2 * step + 1], None)
-            gate_pre = jnp.where(gate_is_own, own, other)
-            up_pre = jnp.where(gate_is_own, other, own)
-            hidden = (jax.nn.silu(gate_pre) * up_pre).astype(jnp.bfloat16)
-            for side in range(2):
-                part = dot_nn(hidden, out_buffer[2 * step + side], None)
-                if step > 0:
-                    part = part + sum_ref[side, here, :]
-                sum_ref[side, here, :] = part
-    for s in range(sets):
-        here = slice(s * rows, (s + 1) * rows)
+    hidden = []
+    for step in range(STEPS):
+        products = []
         for side in range(2):
-            place = (core_ref[0] if side == 0 else 1 - core_ref[0]) * half
-            out_refs[s][:, pl.ds(pl.multiple_of(place, half), half)] = sum_ref[
-                side, here, :
-            ].astype(jnp.bfloat16)
-
-
-def expert_rows(core, row_set, own_in, other_in, own_out, other_out):
+            copy(2 * step + side).wait()
+            products.append(dot_nn(row_ref[...], weight_ref[2 * step + side, :width, :], None))
+        own, other = products
+        gate_pre = jnp.where(gate_is_own, own, other)
+        up_pre = jnp.where(gate_is_own, other, own)
+        hidden.append((jax.nn.silu(gate_pre) * up_pre).astype(jnp.bfloat16))
+    for side in range(2):
+        place = (core_ref[0] if side == 0 else 1 - core_ref[0]) * half
+        for block in range(half // units):
+            top = width + block * units
+            total = None
+            for step in range(STEPS):
+                part = dot_nn(hidden[step], weight_ref[2 * step + side, top : top + units, :], None)
+                total = part if total is None else total + part
+            here = pl.ds(pl.multiple_of(place + block * units, units), units)
+            out_ref[:, here] = total.astype(jnp.bfloat16)
+
+
+def expert_rows(core, row_set, own, other):
     rows, width = row_set.shape
-    units = own_in[0].shape[1]
-    half = own_out[0].shape[1]
+    units = own[0].shape[1]
     vmem = pl.BlockSpec(memory_space=pltpu.VMEM)
     hbm = pl.BlockSpec(memory_space=pl.ANY)
     return pl.pallas_call(
         expert_kernel,
-        in_specs=[pl.BlockSpec(memory_space=pltpu.SMEM), vmem] + [hbm] * 16,
+        in_specs=[pl.BlockSpec(memory_space=pltpu.SMEM), vmem] + [hbm] * (2 * STEPS),
         out_specs=vmem,
         out_shape=jax.ShapeDtypeStruct((rows, width), jnp.bfloat16),
         scratch_shapes=[
-            pltpu.VMEM((8, width, units), jnp.bfloat16),
-            pltpu.VMEM((8, units, half), jnp.bfloat16),
-            pltpu.VMEM((2, rows, half), jnp.float32),
-            pltpu.SemaphoreType.DMA((16,)),
+            pltpu.VMEM((2 * STEPS, *own[0].shape), jnp.bfloat16),
+            pltpu.SemaphoreType.DMA((2 * STEPS,)),
         ],
         cost_estimate=pl.CostEstimate(
-            flops=6 * rows * width * 1024, bytes_accessed=16 * 2**20, transcendentals=0
+            flops=6 * rows * width * units * STEPS,
+            bytes_accessed=16 * 2**20,
+            transcendentals=rows * units * STEPS,
         ),
         name="expert_rows",
-    )(core, row_set, *own_in, *other_in, *own_out, *other_out)
+    )(core, row_set, *[piece for pair in zip(own, other) for piece in pair])
 
 
 def slot_places(slot_count):
@@ -286,21 +279,23 @@
     slots = 2 * devices
     half = model_width // 2
 
-    own_in, own_out, other_in, other_out = [], [], [], []
-    for turn in range(4):
+    own = []
+    for turn in range(STEPS):
         piece = lane ^ turn
         expert, part = piece // 2, piece % 2
         gate_now = lax.dynamic_index_in_dim(w_gate, expert, 0, keepdims=False)
         up_now = lax.dynamic_index_in_dim(w_up, expert, 0, keepdims=False)
         in_now = jnp.where(part == 0, gate_now, up_now)
-        down_now = lax.dynamic_slice(
-            w_down, (expert, 0, part * half), (1, w_down.shape[1], half)
-        )[0]
-        own_in.append(lax.ppermute(in_now, RING, weight_moves(turn)))
-        own_out.append(lax.ppermute(down_now, RING, weight_moves(turn)))
-    for turn in range(4):
-        other_in.append(lax.ppermute(own_in[turn ^ 1], "ep_2", [(0, 1), (1, 0)]))
-        other_out.append(lax.ppermute(own_out[turn ^ 1], "ep_2", [(0, 1), (1, 0)]))
+        units = in_now.shape[1]
+        blocks = [
+            lax.dynamic_slice(w_down, (expert, 0, part * half + k), (1, units, units))[0]
+            for k in range(0, half, units)
+        ]
+        leaving = jnp.concatenate([in_now] + blocks, axis=0)
+        own.append(lax.ppermute(leaving, RING, weight_moves(turn)))
+    other = []
+    for turn in range(STEPS):
+        other.append(lax.ppermute(own[turn ^ 1], "ep_2", [(0, 1), (1, 0)]))
 
     start = lane * qrows
     ids = lax.dynamic_slice_in_dim(expert_ids, start, qrows, 0)
@@ -316,10 +311,8 @@
     results = expert_rows(
         core.astype(jnp.int32).reshape(1),
         arrived.reshape(slots, model_width),
-        own_in,
-        other_in,
-        own_out,
-        other_out,
+        own,
+        other,
     )
 
     returned = lax.all_to_all(
@@ -328,11 +321,9 @@
     returned = returned.reshape(slots, model_width)
     mix = slot_weights(ids, weights, slots)
     high = lax.reduce_precision(mix, 8, 7)
-    out = jnp.dot(high.astype(jnp.bfloat16), returned, preferred_element_type=jnp.float32)
-    out += jnp.dot(
-        (mix - high).astype(jnp.bfloat16), returned, preferred_element_type=jnp.float32
-    )
-    return out.astype(jnp.bfloat16)
+    factors = jnp.concatenate([high, mix - high], axis=0).astype(jnp.bfloat16)
+    sums = jnp.dot(factors, returned, preferred_element_type=jnp.float32)
+    return (sums[:qrows] + sums[qrows:]).astype(jnp.bfloat16)
 
 
 def local(

time: 281 us -> 278 us (0.989)
  starting transfers between devices: 99.2 us -> 90.6 us
  waiting for transfers between devices: 89.4 us -> 93.9 us
  Pallas kernels: 45.2 us -> 49.5 us
  local copies, waits for them, and re-layouts: 24.7 us -> 21.4 us
    ppermute x16 -> x8, starting transfers between devices: 50.2 us -> 41.2 us  [the longest x4 33.4 us: experts(): other.append(lax.ppermute(own[turn ^ 1], 'ep_2', [(0, 1), (1, 0)]))]
    unnamed x0 -> x1, other arithmetic: none -> 4.5 us
    pallas_call x1, Pallas kernels: 12.1 us -> 16.5 us  [expert_rows(): pl.pallas_call(expert_kernel, in_specs=[pl.BlockSpec(memory_space=pltpu.S...]
    ppermute x16 -> x8, waiting for transfers between devices: 43.9 us -> 48.2 us  [the longest x4 48.2 us: experts(): own.append(lax.ppermute(leaving, RING, weight_moves(turn)))]
    select_n x1 -> x0, other arithmetic: 3.84 us -> none  [experts(): in_now = jnp.where(part == 0, gate_now, up_now)]
  transfers between devices with their start and end apart: 23 -> 15, of which waited for: 8 -> 5; matrix products, arithmetic and copies ran while one was open for 11% -> 10% of each run, Pallas kernels for 7% -> 8%
where the time goes in v1:
time: 278 us; the launch traced here: 276 us
  waiting for transfers between devices  93.9 us (34%)
  starting transfers between devices  90.6 us (33%)
  Pallas kernels  49.5 us (18%)
  local copies, waits for them, and re-layouts  21.4 us (8%)
  other arithmetic  11.2 us (4%)
  matrix products  7.74 us (3%)
    ppermute x4, waiting for transfers between devices, experts(): own.append(lax.ppermute(leaving, RING, weight_moves(turn)))  48.2 us
    ppermute x3, waiting for transfers between devices, mixer(): lax.ppermute(part, 'tp', [(i, (i + by) % lanes) for i in range(lanes)])  37.2 us
    ppermute x4, starting transfers between devices, experts(): other.append(lax.ppermute(own[turn ^ 1], 'ep_2', [(0, 1), (1, 0)]))  33.4 us
    pallas_call x1, Pallas kernels, recurrence(): pl.pallas_call(recurrence_kernel, grid=(heads,), in_specs=[wide, wide, wi...  26.5 us
    pallas_call x1, Pallas kernels, expert_rows(): pl.pallas_call(expert_kernel, in_specs=[pl.BlockSpec(memory_space=pltpu.S...  16.5 us
    all_to_all x1, starting transfers between devices, experts(): lax.all_to_all(results.reshape(devices, 2, model_width), EP_TP, 0, 0, til...  12.4 us
    all_to_all x1, starting transfers between devices, mixer(): lax.all_to_all(leaving, EP, split_axis=0, concat_axis=0, tiled=True)  12.1 us
    all_to_all x1, starting transfers between devices, mixer(): starts = lax.all_to_all(before, EP, split_axis=0, concat_axis=0, tiled=True)  9.95 us
  transfers between devices with their start and end apart: 15, of which 5 were waited for; matrix products, arithmetic and copies ran while one was open for 10% of the time, Pallas kernels for 8%

profile of v1, /device:TPU:8, one launch (start us, length us, event | category | flops | bytes accessed | tf_op | source)
XLA Modules:
  0.0 275.5 jit_solution(224440073368077784)
XLA Ops:
  0.6 26.5 %recurrence.1 = (f32[512,512]{1,0:T(8,128)}, f32[512,512]{1,0:T(8,128)}, f32[4,128,128]{2,1,0:T(8,128)}, f32[4,8,128]{2,1,0:T(8,128)}) custom-call(bf16[512,512]{1,0:T(8,128)(2,1)} %q_ref.1, f32[512,512]{1,0:T(8,128)} %f_ref.1, bf16[512,512]{1,0:T(8,128)(2,1)} %v_ref.1, f32[4,1,128]{2,1,0:T(1,128)} %bitcast.56), custom_call_target="tpu_custom_call" | custom-call | tf_op jit(solution)/shard_map/recurrence/pallas_call | solution.py:80
  27.9 1.8 pad_maximum_fusion
  29.7 12.1 %all-to-all-start = ((f32[64,16,128]{2,1,0:T(8,128)}), f32[64,16,128]{2,1,0:T(8,128)S(1)}, u32[]{:S(2)}, u32[]{:S(2)}) async-start(f32[64,16,128]{2,1,0:T(8,128)} %pad_maximum_fusion), calls=%async_computation | async-start | bytes 1048576 | tf_op jit(solution)/shard_map/all_to_all | solution.py:155
  41.8 1.1 fusion.2
  43.2 3.2 %convolution_convert_fusion = bf16[512,2048]{1,0:T(8,128)(2,1)} fusion(pred[512,64]{0,1:T(8,128)(4,1)S(1)} %compare_reduce_fusion.1, f32[2048]{0:T(1024)S(1)} %copy-done.5, f32[64]{0:T(128)S(1)} %add_rsqrt_fusion, bf16[256,2048]{1,0:T(8,128)(2,1)} %param.21, s32[]{:T(128)S(6)} %select_n.306, f32[512]{0:T(512)S(1)} %get-tuple-element.36), kind=kOutput, calls=%fused_computation | convolution fusion | flops 140054528 | bytes 2435588 | tf_op jit(solution)/shard_map/dot_general | solution.py:306
  46.4 4.4 %reshape.241 = bf16[256,2,2048]{2,1,0:T(2,128)(2,1)} reshape(bf16[512,2048]{1,0:T(8,128)(2,1)} %convolution_convert_fusion) | data formatting | bytes 4194304 | tf_op jit(solution)/shard_map/reshape | solution.py:308
  50.8 8.5 %all-to-all-done.pieces_ref = f32[64,16,128]{2,1,0:T(8,128)S(1)} async-done(((f32[64,16,128]{2,1,0:T(8,128)}), f32[64,16,128]{2,1,0:T(8,128)S(1)}, u32[]{:S(2)}, u32[]{:S(2)}) %all-to-all-start) | async-done | bytes 524320 | tf_op jit(solution)/shard_map/all_to_all | solution.py:155
  60.1 9.4 %all-to-all-start.2 = ((bf16[256,2,2048]{2,1,0:T(2,128)(2,1)}), bf16[256,2,2048]{2,1,0:T(2,128)(2,1)}, u32[]{:S(2)}, u32[]{:S(2)}) async-start(bf16[256,2,2048]{2,1,0:T(2,128)(2,1)} %reshape.241), calls=%async_computation.2 | async-start | bytes 4194304 | tf_op jit(solution)/shard_map/all_to_all | solution.py:307
  69.7 4.5 %bitcast_dynamic-update-slice_fusion = (bf16[3072,256]{1,0:T(8,128)(2,1)S(1)}, bf16[3072,256]{1,0:T(8,128)(2,1)S(1)}, bf16[3072,256]{1,0:T(8,128)(2,1)S(1)}, bf16[3072,256]{1,0:T(8,128)(2,1)S(1)}) fusion(bf16[2,2048,256]{2,1,0:T(8,128)(2,1)} %param.26, s32[]{:T(128)S(6)} %select_n.348, bf16[2,2048,256]{2,1,0:T(8,128)(2,1)} %param.25, pred[]{:T(512)S(6)} %eq.83, ...), kind=kLoop, calls=%fused_computation.6 | loop fusion | flops 2097148 | bytes 12582932
  74.6 1.5 collective-permute-start.7
  76.1 1.3 collective-permute-start.4
  77.5 1.8 collective-permute-start.3
  79.3 3.0 %collective-permute-start.8 = (bf16[3072,256]{1,0:T(8,128)(2,1)S(1)}, bf16[3072,256]{1,0:T(8,128)(2,1)}, u32[]{:S(2)}, u32[]{:S(2)}) collective-permute-start(bf16[3072,256]{1,0:T(8,128)(2,1)S(1)} %get-tuple-element.14), channel_id=1, source_target_pairs={{0,5},{1,1},{2,4},{3,0},{4,7},{5,3},{6,6},{7,2},{8,13},{9,9},{10,1... | collective-permute-start | bytes 4718600 | tf_op jit(solution)/shard_map/ppermute | solution.py:295
  82.3 48.1 %collective-permute-done.7.refs_4_ = bf16[3072,256]{1,0:T(8,128)(2,1)} collective-permute-done((bf16[3072,256]{1,0:T(8,128)(2,1)S(1)}, bf16[3072,256]{1,0:T(8,128)(2,1)}, u32[]{:S(2)}, u32[]{:S(2)}) %collective-permute-start.7) | collective-permute-done | bytes 1572896 | tf_op jit(solution)/shard_map/ppermute | solution.py:295
  130.9 32.3 %collective-permute-start.6 = (bf16[3072,256]{1,0:T(8,128)(2,1)}, bf16[3072,256]{1,0:T(8,128)(2,1)}, u32[]{:S(2)}, u32[]{:S(2)}) collective-permute-start(bf16[3072,256]{1,0:T(8,128)(2,1)} %collective-permute-done.3.refs_0_), channel_id=1, source_target_pairs={{0,4},{4,0},{1,5},{5,1},{2,6},{6,2},{3,7},{7,3},{8,12},{12,8},{9,1... | collective-permute-start | bytes 4718600 | tf_op jit(solution)/shard_map/ppermute | solution.py:298
  163.9 2.1 prefix.1
  166.1 10.0 %all-to-all-start.1 = ((f32[64,8,128]{2,1,0:T(8,128)}), f32[64,8,128]{2,1,0:T(8,128)S(1)}, u32[]{:S(2)}, u32[]{:S(2)}) async-start(f32[64,8,128]{2,1,0:T(8,128)} %prefix.1), calls=%async_computation.1 | async-start | bytes 524288 | tf_op jit(solution)/shard_map/all_to_all | solution.py:157
  176.1 4.1 %reshape.242.row_ref = bf16[512,2048]{1,0:T(8,128)(2,1)} reshape(bf16[256,2,2048]{2,1,0:T(2,128)(2,1)} %all-to-all-done.2) | data formatting | bytes 4194304 | tf_op jit(solution)/shard_map/reshape | solution.py:313
  180.2 16.5 %expert_rows.1 = bf16[512,2048]{1,0:T(8,128)(2,1)} custom-call(s32[1]{0:T(128)} %bitcast.5.core_ref, bf16[512,2048]{1,0:T(8,128)(2,1)} %reshape.242.row_ref, bf16[3072,256]{1,0:T(8,128)(2,1)} %collective-permute-done.3.refs_0_, bf16[3072,256]{1,0:T(8,128)(2,1)} %collective-permute-done.5.refs_1_, bf16[3072,256]{1,0:T(8,128)(2,1)} %collective-permute-done.4.refs_2_, ...), custom_call_target="tpu_custom_call" | custom-call | flops 6442450944 | bytes 16777216 | tf_op jit(solution)/shard_map/expert_rows/pallas_call | solution.py:215
  196.7 4.4 %reshape.243 = bf16[256,2,2048]{2,1,0:T(2,128)(2,1)} reshape(bf16[512,2048]{1,0:T(8,128)(2,1)} %expert_rows.1) | data formatting | bytes 4194304 | tf_op jit(solution)/shard_map/reshape | solution.py:319
  201.7 12.4 %all-to-all-start.3 = ((bf16[256,2,2048]{2,1,0:T(2,128)(2,1)}), bf16[256,2,2048]{2,1,0:T(2,128)(2,1)}, u32[]{:S(2)}, u32[]{:S(2)}) async-start(bf16[256,2,2048]{2,1,0:T(2,128)(2,1)} %reshape.243), calls=%async_computation.3 | async-start | bytes 4194304 | tf_op jit(solution)/shard_map/all_to_all | solution.py:318
  214.3 4.5 %gate.1 = bf16[512,512]{1,0:T(8,128)(2,1)} custom-call(f32[512,512]{1,0:T(8,128)} %get-tuple-element.6.rec_ref, f32[512,512]{1,0:T(8,128)} %get-tuple-element.7.query_ref, f32[4,128,128]{2,1,0:T(8,128)} %bitcast.53, bf16[512,512]{1,0:T(8,128)(2,1)} %out_gate_ref.1, f32[1,128]{1,0:T(1,128)} %bitcast.57), custom_call_target="tpu_custom_call" | custom-call | tf_op jit(solution)/shard_map/gate/pallas_call | solution.py:125
  218.8 2.3 convolution_convert_fusion.1
  221.1 1.0 constant_dynamic-slice_fusion.4
  222.6 1.5 collective-permute-start
  224.1 2.7 collective-permute-start.1
  226.8 1.5 collective-permute-start.2
  228.8 18.0 %collective-permute-done = bf16[128,2048]{1,0:T(8,128)(2,1)} collective-permute-done((bf16[128,2048]{1,0:T(8,128)(2,1)}, bf16[128,2048]{1,0:T(8,128)(2,1)}, u32[]{:S(2)}, u32[]{:S(2)}) %collective-permute-start) | collective-permute-done | bytes 524320 | tf_op jit(solution)/shard_map/ppermute | solution.py:166
  246.8 19.2 %collective-permute-done.1 = bf16[128,2048]{1,0:T(8,128)(2,1)} collective-permute-done((bf16[128,2048]{1,0:T(8,128)(2,1)S(1)}, bf16[128,2048]{1,0:T(8,128)(2,1)}, u32[]{:S(2)}, u32[]{:S(2)}) %collective-permute-start.1) | collective-permute-done | bytes 524320 | tf_op jit(solution)/shard_map/ppermute | solution.py:166
  266.0 2.6 add_convert_fusion
  268.6 4.1 %reshape.244 = bf16[512,2048]{1,0:T(8,128)(2,1)} reshape(bf16[256,2,2048]{2,1,0:T(2,128)(2,1)} %all-to-all-done.3) | data formatting | bytes 4194304 | tf_op jit(solution)/shard_map/reshape | solution.py:321
  272.7 2.0 fusion.12
  (45 shorter events, 5.9 us)
Async XLA Ops:
  0.6 218.1 %copy-start = (bf16[512,2048]{1,0:T(8,128)(2,1)S(1)}, bf16[512,2048]{1,0:T(8,128)(2,1)}, u32[]{:S(2)}) copy-start(bf16[512,2048]{1,0:T(8,128)(2,1)} %param.20) | copy-start | bytes 6291460
  27.1 15.8 %copy-start.6 = (s32[256,4]{0,1:T(4,128)S(1)}, s32[256,4]{0,1:T(4,128)}, u32[]{:S(2)}) copy-start(s32[256,4]{0,1:T(4,128)} %param.23) | copy-start | bytes 12292
  27.1 16.1 %copy-start.5 = (f32[2048]{0:T(1024)S(1)}, f32[2048]{0:T(1024)}, u32[]{:S(2)}) copy-start(f32[2048]{0:T(1024)} %param.22) | copy-start | bytes 24580
  29.7 29.6 %all-to-all-start = ((f32[64,16,128]{2,1,0:T(8,128)}), f32[64,16,128]{2,1,0:T(8,128)S(1)}, u32[]{:S(2)}, u32[]{:S(2)}) async-start(f32[64,16,128]{2,1,0:T(8,128)} %pad_maximum_fusion), calls=%async_computation | async-start | bytes 1048576 | tf_op jit(solution)/shard_map/all_to_all | solution.py:155
  59.3 0.8 copy-start.3
  60.1 106.0 %all-to-all-start.2 = ((bf16[256,2,2048]{2,1,0:T(2,128)(2,1)}), bf16[256,2,2048]{2,1,0:T(2,128)(2,1)}, u32[]{:S(2)}, u32[]{:S(2)}) async-start(bf16[256,2,2048]{2,1,0:T(2,128)(2,1)} %reshape.241), calls=%async_computation.2 | async-start | bytes 4194304 | tf_op jit(solution)/shard_map/all_to_all | solution.py:307
  69.7 4.5 %copy-start.1 = (bf16[2,256,2048]{2,1,0:T(8,128)(2,1)S(1)}, bf16[2,256,2048]{2,1,0:T(8,128)(2,1)}, u32[]{:S(2)}) copy-start(bf16[2,256,2048]{2,1,0:T(8,128)(2,1)} %param.27) | copy-start | bytes 6291460
  74.6 55.8 %collective-permute-start.7 = (bf16[3072,256]{1,0:T(8,128)(2,1)S(1)}, bf16[3072,256]{1,0:T(8,128)(2,1)}, u32[]{:S(2)}, u32[]{:S(2)}) collective-permute-start(bf16[3072,256]{1,0:T(8,128)(2,1)S(1)} %get-tuple-element.15), channel_id=1, source_target_pairs={{0,1},{1,5},{2,0},{3,4},{4,3},{5,7},{6,2},{7,6},{8,9},{9,13},{10,8... | collective-permute-start | bytes 4718600 | tf_op jit(solution)/shard_map/ppermute | solution.py:295
  76.1 54.3 %collective-permute-start.4 = (bf16[3072,256]{1,0:T(8,128)(2,1)S(1)}, bf16[3072,256]{1,0:T(8,128)(2,1)}, u32[]{:S(2)}, u32[]{:S(2)}) collective-permute-start(bf16[3072,256]{1,0:T(8,128)(2,1)S(1)} %get-tuple-element.16), channel_id=1, source_target_pairs={{0,4},{1,0},{2,5},{3,1},{4,6},{5,2},{6,7},{7,3},{8,12},{9,8},{10,1... | collective-permute-start | bytes 4718600 | tf_op jit(solution)/shard_map/ppermute | solution.py:295
  77.5 53.5 %collective-permute-start.3 = (bf16[3072,256]{1,0:T(8,128)(2,1)S(1)}, bf16[3072,256]{1,0:T(8,128)(2,1)}, u32[]{:S(2)}, u32[]{:S(2)}) collective-permute-start(bf16[3072,256]{1,0:T(8,128)(2,1)S(1)} %get-tuple-element.17), channel_id=1, source_target_pairs={{0,0},{1,4},{2,1},{3,5},{4,2},{5,6},{6,3},{7,7},{8,8},{9,12},{10,9... | collective-permute-start | bytes 4718600 | tf_op jit(solution)/shard_map/ppermute | solution.py:295
  79.3 84.1 %collective-permute-start.8 = (bf16[3072,256]{1,0:T(8,128)(2,1)S(1)}, bf16[3072,256]{1,0:T(8,128)(2,1)}, u32[]{:S(2)}, u32[]{:S(2)}) collective-permute-start(bf16[3072,256]{1,0:T(8,128)(2,1)S(1)} %get-tuple-element.14), channel_id=1, source_target_pairs={{0,5},{1,1},{2,4},{3,0},{4,7},{5,3},{6,6},{7,2},{8,13},{9,9},{10,1... | collective-permute-start | bytes 4718600 | tf_op jit(solution)/shard_map/ppermute | solution.py:295
  130.4 49.7 %collective-permute-start.10 = (bf16[3072,256]{1,0:T(8,128)(2,1)}, bf16[3072,256]{1,0:T(8,128)(2,1)}, u32[]{:S(2)}, u32[]{:S(2)}) collective-permute-start(bf16[3072,256]{1,0:T(8,128)(2,1)} %collective-permute-done.7.refs_4_), channel_id=1, source_target_pairs={{0,4},{4,0},{1,5},{5,1},{2,6},{6,2},{3,7},{7,3},{8,12},{12,8},{9,1... | collective-permute-start | bytes 4718600 | tf_op jit(solution)/shard_map/ppermute | solution.py:298
  130.4 49.7 %collective-permute-start.5 = (bf16[3072,256]{1,0:T(8,128)(2,1)}, bf16[3072,256]{1,0:T(8,128)(2,1)}, u32[]{:S(2)}, u32[]{:S(2)}) collective-permute-start(bf16[3072,256]{1,0:T(8,128)(2,1)} %collective-permute-done.4.refs_2_), channel_id=1, source_target_pairs={{0,4},{4,0},{1,5},{5,1},{2,6},{6,2},{3,7},{7,3},{8,12},{12,8},{9,1... | collective-permute-start | bytes 4718600 | tf_op jit(solution)/shard_map/ppermute | solution.py:298
  130.9 49.2 %collective-permute-start.6 = (bf16[3072,256]{1,0:T(8,128)(2,1)}, bf16[3072,256]{1,0:T(8,128)(2,1)}, u32[]{:S(2)}, u32[]{:S(2)}) collective-permute-start(bf16[3072,256]{1,0:T(8,128)(2,1)} %collective-permute-done.3.refs_0_), channel_id=1, source_target_pairs={{0,4},{4,0},{1,5},{5,1},{2,6},{6,2},{3,7},{7,3},{8,12},{12,8},{9,1... | collective-permute-start | bytes 4718600 | tf_op jit(solution)/shard_map/ppermute | solution.py:298
  163.4 16.8 %collective-permute-start.9 = (bf16[3072,256]{1,0:T(8,128)(2,1)}, bf16[3072,256]{1,0:T(8,128)(2,1)}, u32[]{:S(2)}, u32[]{:S(2)}) collective-permute-start(bf16[3072,256]{1,0:T(8,128)(2,1)} %collective-permute-done.8.refs_6_), channel_id=1, source_target_pairs={{0,4},{4,0},{1,5},{5,1},{2,6},{6,2},{3,7},{7,3},{8,12},{12,8},{9,1... | collective-permute-start | bytes 4718600 | tf_op jit(solution)/shard_map/ppermute | solution.py:298
  166.1 34.9 %all-to-all-start.1 = ((f32[64,8,128]{2,1,0:T(8,128)}), f32[64,8,128]{2,1,0:T(8,128)S(1)}, u32[]{:S(2)}, u32[]{:S(2)}) async-start(f32[64,8,128]{2,1,0:T(8,128)} %prefix.1), calls=%async_computation.1 | async-start | bytes 524288 | tf_op jit(solution)/shard_map/all_to_all | solution.py:157
  201.0 0.7 copy-start.4
  201.7 66.9 %all-to-all-start.3 = ((bf16[256,2,2048]{2,1,0:T(2,128)(2,1)}), bf16[256,2,2048]{2,1,0:T(2,128)(2,1)}, u32[]{:S(2)}, u32[]{:S(2)}) async-start(bf16[256,2,2048]{2,1,0:T(2,128)(2,1)} %reshape.243), calls=%async_computation.3 | async-start | bytes 4194304 | tf_op jit(solution)/shard_map/all_to_all | solution.py:318
  221.1 1.6 copy-start.2
  221.1 7.2 %copy-start.7 = (f32[256,4]{0,1:T(4,128)S(1)}, f32[256,4]{0,1:T(4,128)}, u32[]{:S(2)}) copy-start(f32[256,4]{0,1:T(4,128)} %param.24) | copy-start | bytes 12292
  222.6 24.1 %collective-permute-start = (bf16[128,2048]{1,0:T(8,128)(2,1)}, bf16[128,2048]{1,0:T(8,128)(2,1)}, u32[]{:S(2)}, u32[]{:S(2)}) collective-permute-start(bf16[128,2048]{1,0:T(8,128)(2,1)} %get-tuple-element.30), channel_id=1, source_target_pairs={{0,1},{1,2},{2,3},{3,0},{4,5},{5,6},{6,7},{7,4},{8,9},{9,10},{10,1... | collective-permute-start | bytes 1572872 | tf_op jit(solution)/shard_map/ppermute | solution.py:166
  224.1 41.9 %collective-permute-start.1 = (bf16[128,2048]{1,0:T(8,128)(2,1)S(1)}, bf16[128,2048]{1,0:T(8,128)(2,1)}, u32[]{:S(2)}, u32[]{:S(2)}) collective-permute-start(bf16[128,2048]{1,0:T(8,128)(2,1)S(1)} %get-tuple-element.32), channel_id=1, source_target_pairs={{0,2},{1,3},{2,0},{3,1},{4,6},{5,7},{6,4},{7,5},{8,10},{9,11},{10,... | collective-permute-start | bytes 1572872 | tf_op jit(solution)/shard_map/ppermute | solution.py:166
  226.8 39.2 %collective-permute-start.2 = (bf16[128,2048]{1,0:T(8,128)(2,1)S(1)}, bf16[128,2048]{1,0:T(8,128)(2,1)}, u32[]{:S(2)}, u32[]{:S(2)}) collective-permute-start(bf16[128,2048]{1,0:T(8,128)(2,1)S(1)} %get-tuple-element.31), channel_id=1, source_target_pairs={{0,3},{1,0},{2,1},{3,2},{4,7},{5,4},{6,5},{7,6},{8,11},{9,8},{10,9... | collective-permute-start | bytes 1572872 | tf_op jit(solution)/shard_map/ppermute | solution.py:166
